TPU v7x, 32 devices: a whole 2x2x4 slice. The times are simulated.
32 devices in a mesh: ra: 2 (over core), cb: 4 (over z), dp: 4 (over y, x).
Axes of the slice: x: 2, y: 2, z: 4, core: 2. Of those that a mesh axis runs over, the one named last changes fastest.
Arguments:
- residual_in: bfloat16 [1024, 4096], P('dp', 'cb'), may hold values from -220 to 220, as said below
- gain_in: float32 [4096], P('cb'), may hold values from 0.1 to 1.9
- shift_in: float32 [4096], P('cb'), may hold values from -3 to 3
- up_weight: bfloat16 [4096, 16384], P('cb', 'ra'), may hold values from -0.09375 to 0.09375
- down_weight: bfloat16 [16384, 4096], P('ra', 'cb'), may hold values from -0.046875 to 0.046875
- gain_out: float32 [4096], P('cb'), may hold values from 0.1 to 1.9
- shift_out: float32 [4096], P('cb'), may hold values from -3 to 3
Outputs:
- layer_out: bfloat16 [1024, 4096], P('dp', 'cb')
Inputs may be any that keep to these rules, and one draw needn't show every extreme that they name: `residual_in`: real-valued activations.
All inputs are finite; a program needn't handle non-finite values.
Results may differ from a plain program's by a relative error of at most 0.0065.
Values may be sent and summed in bfloat16 or wider, within the bound.
A program may use at most 128 MiB of HBM per device.

v0:
```python
import jax
import jax.numpy as jnp
from jax import lax
from jax.sharding import PartitionSpec as P


def standardize(values):
    count = values.shape[1] * lax.axis_size("cb")
    sums = lax.psum(jnp.sum(values, axis=1), "cb")
    mean = sums / count
    centred = values - mean[:, None]
    spread = lax.psum(jnp.sum(centred * centred, axis=1), "cb") / count
    return (values - mean[:, None]) * lax.rsqrt(spread + 1e-05)[:, None]


def per_device(residual_in, gain_in, shift_in, up_weight, down_weight, gain_out, shift_out):
    normed = (standardize(residual_in.astype(jnp.float32)) * gain_in + shift_in).astype(
        jnp.bfloat16
    )
    products = jnp.dot(normed, up_weight, preferred_element_type=jnp.float32)
    share = lax.psum_scatter(products, "cb", scatter_dimension=1, tiled=True)
    hidden_share = jnp.square(jax.nn.relu(share)).astype(jnp.bfloat16)
    branch_part = jnp.dot(
        lax.all_gather(hidden_share, "cb", axis=1, tiled=True),
        down_weight,
        preferred_element_type=jnp.float32,
    )
    branch = lax.psum(branch_part, "ra")
    total = 2.0**0.25 * normed.astype(jnp.float32) + branch
    return (standardize(total) * gain_out + shift_out).astype(jnp.bfloat16)


def solution(mesh):
    in_specs = (P("dp", "cb"), P("cb"), P("cb"), P("cb", "ra"), P("ra", "cb"), P("cb"), P("cb"))
    out_specs = P("dp", "cb")
    return jax.shard_map(
        per_device, mesh=mesh, in_specs=in_specs, out_specs=out_specs, check_vma=False
    )
```

profile of v0, /device:TPU:0, one launch (start us, length us, event | category | flops | bytes accessed | tf_op | source)
XLA Modules:
  0.0 337.2 jit_solution(11542523909155165681)
XLA Ops:
  6.5 1.2 convert_reduce_fusion
  7.7 13.5 %psum.35 = f32[256]{0:T(256)S(1)} all-reduce(f32[256]{0:T(256)S(1)} %convert_reduce_fusion), channel_id=1, replica_groups=mesh['ra'=2,'cb'=4,'dp'=4] {'cb'}, use_global_device_ids=true, to_apply=%region_1.0 | all-reduce | flops 256 | bytes 2048 | tf_op jit(solution)/shard_map/psum | solution.py:9
  21.2 1.3 fusion.2
  22.5 8.4 %psum.36 = f32[256]{0:T(256)S(1)} all-reduce(f32[256]{0:T(256)S(1)} %fusion.2), channel_id=1, replica_groups=mesh['ra'=2,'cb'=4,'dp'=4] {'cb'}, use_global_device_ids=true, to_apply=%region_3.0 | all-reduce | flops 256 | bytes 2048 | tf_op jit(solution)/shard_map/psum | solution.py:12
  30.9 13.8 %fusion.7 = f32[256,8192]{1,0:T(8,128)} fusion(bf16[1024,8192]{1,0:T(8,128)(2,1)} %param.10, bf16[256,1024]{1,0:T(8,128)(2,1)} %param.7, f32[1024]{0:T(1024)} %param.9, f32[1024]{0:T(1024)} %param.8, f32[256]{0:T(256)S(1)} %add_rsqrt_fusion.1, f32[256]{0:T(256)S(1)} %broadcast_multiply_fusion.1), kind=kOutput, calls=%fused_computation.17 | convolution fusion | flops 4296540160 | bytes 25700352 | tf_op jit(solution)/shard_map/dot_general | solution.py:20
  44.8 0.0 reduce-scatter.2.cloned.1.call-update
  44.8 0.0 all-gather.2.cloned.1.call-start
  44.8 144.4 %reduce-scatter.2.cloned.1.call-done = f32[256,2048]{1,0:T(8,128)} async-done(((f32[256,8192]{1,0:T(8,128)}), f32[256,2048]{1,0:T(8,128)}) %reduce-scatter.2.cloned.1.call-update) | async-done | bytes 2097168 | tf_op jit(solution)/shard_map/reduce_scatter | solution.py:21
  189.2 2.8 multiply_convert_fusion
  192.0 0.0 all-gather.2.cloned.1.call-update
  192.0 0.0 copy-start
  192.0 0.0 copy-start.1
  192.1 0.0 copy-start.2
  192.1 0.0 copy-start.3
  192.1 0.0 all-reduce.2.cloned.1.call-start
  192.1 81.4 %all-gather.2.cloned.1.call-done = bf16[256,8192]{1,0:T(8,128)(2,1)} async-done(((bf16[256,2048]{1,0:T(8,128)(2,1)}), bf16[256,8192]{1,0:T(8,128)(2,1)}) %all-gather.2.cloned.1.call-update) | async-done | bytes 4194320 | tf_op jit(solution)/shard_map/all_gather | solution.py:24
  273.5 12.5 %fusion.9 = f32[256,1024]{1,0:T(8,128)} fusion(bf16[256,8192]{1,0:T(8,128)(2,1)} %all-gather.2.cloned.1.call-done, bf16[8192,1024]{1,0:T(8,128)(2,1)} %param.11), kind=kOutput, calls=%fused_computation.18 | convolution fusion | flops 4294967296 | bytes 22020096 | tf_op jit(solution)/shard_map/dot_general | solution.py:23
  286.0 0.0 all-reduce.2.cloned.1.call-update
  286.1 18.1 %all-reduce.2.cloned.1.call-done = f32[256,1024]{1,0:T(8,128)} async-done(((f32[256,1024]{1,0:T(8,128)}), f32[256,1024]{1,0:T(8,128)}) %all-reduce.2.cloned.1.call-update) | async-done | bytes 1048592 | tf_op jit(solution)/shard_map/psum | solution.py:28
  304.1 1.7 fusion.6
  305.8 12.0 %psum.38 = f32[256]{0:T(256)S(1)} all-reduce(f32[256]{0:T(256)S(1)} %fusion.6), channel_id=1, replica_groups=mesh['ra'=2,'cb'=4,'dp'=4] {'cb'}, use_global_device_ids=true, to_apply=%region_7.8 | all-reduce | flops 256 | bytes 2048 | tf_op jit(solution)/shard_map/psum | solution.py:9
  317.8 1.7 multiply_reduce_fusion
  319.5 8.4 %psum.39 = f32[256]{0:T(256)S(1)} all-reduce(f32[256]{0:T(256)S(1)} %multiply_reduce_fusion), channel_id=1, replica_groups=mesh['ra'=2,'cb'=4,'dp'=4] {'cb'}, use_global_device_ids=true, to_apply=%region_9.10 | all-reduce | flops 256 | bytes 2048 | tf_op jit(solution)/shard_map/psum | solution.py:12
  327.9 2.8 add_convert_fusion
  (11 shorter events, 0.0 us)
Async XLA Ops:
  6.5 182.7 %reduce-scatter.2.cloned.1.call-start = ((), (), s32[]{:S(2)}) async-start(), calls=%async_computation.1 | async-start | bytes 10485760 | tf_op jit(solution)/shard_map/reduce_scatter | solution.py:21
  44.8 228.8 %all-gather.2.cloned.1.call-start = ((), (), s32[]{:S(2)}) async-start(), calls=%async_computation.2 | async-start | bytes 5242880 | tf_op jit(solution)/shard_map/all_gather | solution.py:24
  192.0 112.1 %copy-start = (bf16[256,1024]{1,0:T(8,128)(2,1)S(1)}, bf16[256,1024]{1,0:T(8,128)(2,1)}, u32[]{:S(2)}) copy-start(bf16[256,1024]{1,0:T(8,128)(2,1)} %param.7) | copy-start | bytes 1572868
  192.0 112.1 %copy-start.1 = (f32[1024]{0:T(1024)S(1)}, f32[1024]{0:T(1024)}, u32[]{:S(2)}) copy-start(f32[1024]{0:T(1024)} %param.9) | copy-start | bytes 12292
  192.1 112.1 %copy-start.2 = (f32[1024]{0:T(1024)S(1)}, f32[1024]{0:T(1024)}, u32[]{:S(2)}) copy-start(f32[1024]{0:T(1024)} %param.8) | copy-start | bytes 12292
  192.1 135.8 %copy-start.3 = (f32[1024]{0:T(1024)S(1)}, f32[1024]{0:T(1024)}, u32[]{:S(2)}) copy-start(f32[1024]{0:T(1024)} %param.13) | copy-start | bytes 12292
  192.1 135.8 %copy-start.4 = (f32[1024]{0:T(1024)S(1)}, f32[1024]{0:T(1024)}, u32[]{:S(2)}) copy-start(f32[1024]{0:T(1024)} %param.12) | copy-start | bytes 12292
  192.1 112.0 %all-reduce.2.cloned.1.call-start = ((), (), s32[]{:S(2)}) async-start(), calls=%async_computation.3 | async-start | bytes 2097152 | tf_op jit(solution)/shard_map/psum | solution.py:28
Sparse Core Ops, SparseCore 0:
  44.9 144.2 reduce-scatter.1
  192.2 81.3 all-gather.1
  286.2 17.8 all-reduce.1
where the time goes:
time: 338 us; the launch traced here: 337 us
  waiting for transfers between devices  244 us (72%)
  blocking collectives  42.2 us (12%)
  matrix products  26.3 us (8%)
  between operations  13.2 us (4%)
  other arithmetic  11.5 us (3%)
    reduce_scatter x1, waiting for transfers between devices, per_device(): share = lax.psum_scatter(products, 'cb', scatter_dimension=1, tiled=True)  144 us
    all_gather x1, waiting for transfers between devices, per_device(): lax.all_gather(hidden_share, 'cb', axis=1, tiled=True)  81.4 us
    psum x2, blocking collectives, standardize(): sums = lax.psum(jnp.sum(values, axis=1), 'cb')  25.5 us
    psum x1, waiting for transfers between devices, per_device(): branch = lax.psum(branch_part, 'ra')  18.1 us
    psum x2, blocking collectives, standardize(): spread = lax.psum(jnp.sum(centred * centred, axis=1), 'cb') / count  16.7 us
    dot_general x1, matrix products, per_device(): products = jnp.dot(normed, up_weight, preferred_element_type=jnp.float32)  13.8 us
    dot_general x1, matrix products, per_device(): jnp.dot(lax.all_gather(hidden_share, 'cb', axis=1, tiled=True), down_weig...  12.5 us
  transfers between devices with their start and end apart: 3, of which 3 were waited for; matrix products, arithmetic and copies ran while one was open for 0% of the time, Pallas kernels for 0%

commit v1 on v0

v1 whole, which is shorter than its diff:
```python
import functools

import jax
import jax.numpy as jnp
from jax import lax
from jax.experimental import pallas as pl
from jax.experimental.pallas import tpu as pltpu
from jax.sharding import PartitionSpec as P

MESH = pl.DeviceIdType.MESH
LANES = 128
STAT_ROWS = 8
CHUNK = 256
WINDOW = 3
LAG = 2
LAG_STEP = 4


def kernel(
    n, n_ra, x_ref, gain_in_ref, shift_in_ref, gain_out_ref, shift_out_ref, up_hbm, down_hbm, out_ref,
    up_v, down_v, sums, from_outer, from_partner, hidden, normed, acc, acc_in, stats_in, stats_out,
    up_sem, down_sem, sums_sent, outer_got, partner_got, hidden_sent, hidden_got,
    stat_sent, stat_got, acc_sent, acc_got,
):
    me = lax.axis_index("cb")
    ra = lax.axis_index("ra")
    chunks, depth, width = up_v.shape
    tokens = x_ref.shape[0]
    half = n // 2
    side = me // half
    level = me * (1 - side) + (n - 1 - me) * side
    inner = lax.rem(me + 1 - 2 * side + n, n)
    outer = lax.rem(me - 1 + 2 * side + n, n)
    is_mid = level == half - 1
    has_outer = level > 0

    def up_copy(c):
        columns = pl.ds(pl.multiple_of(c * width, width), width)
        return pltpu.make_async_copy(up_hbm.at[:, columns], up_v.at[c], up_sem.at[c])

    def down_copy(c):
        rows = pl.ds(pl.multiple_of(c * width, width), width)
        return pltpu.make_async_copy(down_hbm.at[rows, :], down_v.at[c], down_sem.at[c])

    @pl.loop(0, chunks)
    def _(c):
        up_copy(c).start()

    @pl.loop(0, chunks)
    def _(c):
        down_copy(c).start()

    barrier = pltpu.get_barrier_semaphore()
    for k in range(1, n):
        pl.semaphore_signal(barrier, inc=1, device_id={"cb": lax.rem(me + k, n)}, device_id_type=MESH)
    for k in range(1, n_ra):
        pl.semaphore_signal(barrier, inc=1, device_id={"ra": lax.rem(ra + k, n_ra)}, device_id_type=MESH)

    def local_stats(values, stats):
        total = jnp.sum(values, axis=1, keepdims=True)
        centred = values - total * (1.0 / depth)
        squares = jnp.sum(centred * centred, axis=1, keepdims=True)
        lane = lax.broadcasted_iota(jnp.int32, (tokens, LANES), 1)
        tile = jnp.where(lane == 0, total, jnp.where(lane == 1, squares, 0.0))
        stats[me] = tile.T[:STAT_ROWS]

    def stat_copy(stats, which, k, slot):
        return pltpu.make_async_remote_copy(
            src_ref=stats.at[slot], dst_ref=stats.at[slot],
            send_sem=stat_sent.at[which, k], recv_sem=stat_got.at[which, slot],
            device_id={"cb": lax.rem(me + k, n)}, device_id_type=MESH,
        )

    def send_stats(stats, which):
        for k in range(1, n):
            stat_copy(stats, which, k, me).start()

    def merged_stats(stats, which):
        for k in range(1, n):
            stat_copy(stats, which, k, lax.rem(me + k, n)).wait_recv()
        for k in range(1, n):
            stat_copy(stats, which, k, me).wait_send()
        total = stats[0][0:1]
        for j in range(1, n):
            total = total + stats[j][0:1]
        mean = total / (depth * n)
        squares = jnp.zeros_like(mean)
        for j in range(n):
            block = stats[j]
            gap = block[0:1] * (1.0 / depth) - mean
            squares = squares + (block[1:2] + depth * (gap * gap))
        scale = lax.rsqrt(squares / (depth * n) + 1e-05)
        row = lax.broadcasted_iota(jnp.int32, (LANES, tokens), 0)
        tile = jnp.where(row == 0, mean, jnp.where(row == 1, scale, 0.0)).T
        return tile[:, 0:1], tile[:, 1:2]

    values = x_ref[...].astype(jnp.float32)
    local_stats(values, stats_in)
    acc[...] = jnp.zeros_like(acc)
    pl.semaphore_wait(barrier, n - 1 + n_ra - 1)
    send_stats(stats_in, 0)
    mean, scale = merged_stats(stats_in, 0)
    normed[...] = (
        (x_ref[...].astype(jnp.float32) - mean) * scale * gain_in_ref[...] + shift_in_ref[...]
    ).astype(jnp.bfloat16)

    def sum_copy(c, into, got):
        return pltpu.make_async_remote_copy(
            src_ref=sums.at[c], dst_ref=into.at[c], send_sem=sums_sent.at[c], recv_sem=got.at[c],
            device_id={"cb": inner}, device_id_type=MESH,
        )

    def hidden_copy(c):
        return pltpu.make_async_remote_copy(
            src_ref=hidden.at[c], dst_ref=hidden.at[c], send_sem=hidden_sent.at[c],
            recv_sem=hidden_got.at[c], device_id={"cb": outer}, device_id_type=MESH,
        )

    def inward(c):
        up_copy(c).wait()
        part = jnp.dot(normed[...], up_v[c], preferred_element_type=jnp.float32)

        @pl.when(has_outer)
        def _():
            sum_copy(c, from_outer, outer_got).wait_recv()
            sums[c] = (part + from_outer[c].astype(jnp.float32)).astype(jnp.bfloat16)

        @pl.when(level == 0)
        def _():
            sums[c] = part.astype(jnp.bfloat16)

        @pl.when(c >= WINDOW)
        def _():
            sum_copy(c - WINDOW, from_outer, outer_got).wait_send()

        @pl.when(is_mid)
        def _():
            sum_copy(c, from_partner, partner_got).start()

        @pl.when(level < half - 1)
        def _():
            sum_copy(c, from_outer, outer_got).start()

    def outward(c):
        @pl.when(is_mid)
        def _():
            sum_copy(c, from_partner, partner_got).wait_recv()
            full = sums[c].astype(jnp.float32) + from_partner[c].astype(jnp.float32)
            hidden[c] = jnp.square(jnp.maximum(full, 0.0)).astype(jnp.bfloat16)

        @pl.when(level < half - 1)
        def _():
            hidden_copy(c).wait_recv()

        @pl.when(has_outer)
        def _():
            hidden_copy(c).start()

        down_copy(c).wait()
        acc[...] += jnp.dot(hidden[c], down_v[c], preferred_element_type=jnp.float32)

    lag = LAG + LAG_STEP * (half - 1 - level)

    @pl.loop(0, chunks + lag)
    def _(step):
        @pl.when(step < chunks)
        def _():
            inward(step)

        @pl.when(step >= lag)
        def _():
            outward(step - lag)

    def acc_copy(k):
        return pltpu.make_async_remote_copy(
            src_ref=acc, dst_ref=acc_in.at[k - 1], send_sem=acc_sent.at[k - 1], recv_sem=acc_got.at[k - 1],
            device_id={"ra": lax.rem(ra + k, n_ra)}, device_id_type=MESH,
        )

    for k in range(1, n_ra):
        acc_copy(k).start()

    @pl.loop(max(chunks - WINDOW, 0), chunks)
    def _(c):
        sum_copy(c, from_outer, outer_got).wait_send()

    @pl.when(has_outer)
    def _():
        @pl.loop(0, chunks)
        def _(c):
            hidden_copy(c).wait_send()

    for k in range(1, n_ra):
        acc_copy(k).wait()
    branch = acc[...]
    for k in range(1, n_ra):
        branch = branch + acc_in[k - 1]
    total = 2.0**0.25 * normed[...].astype(jnp.float32) + branch
    acc[...] = total
    local_stats(total, stats_out)
    send_stats(stats_out, 1)
    mean, scale = merged_stats(stats_out, 1)
    out_ref[...] = ((acc[...] - mean) * scale * gain_out_ref[...] + shift_out_ref[...]).astype(jnp.bfloat16)


def solution(mesh):
    n, n_ra = mesh.shape["cb"], mesh.shape["ra"]

    def per_device(residual_in, gain_in, shift_in, up_weight, down_weight, gain_out, shift_out):
        tokens, depth = residual_in.shape
        units = up_weight.shape[1]
        width = CHUNK if units % CHUNK == 0 else units
        chunks = units // width
        vmem = pl.BlockSpec(memory_space=pltpu.VMEM)
        hbm = pl.BlockSpec(memory_space=pl.ANY)
        block = (chunks, tokens, width)
        return pl.pallas_call(
            functools.partial(kernel, n, n_ra),
            out_shape=jax.ShapeDtypeStruct((tokens, depth), jnp.bfloat16),
            in_specs=[vmem] * 5 + [hbm] * 2,
            out_specs=vmem,
            scratch_shapes=[
                pltpu.VMEM((chunks, depth, width), jnp.bfloat16),
                pltpu.VMEM((chunks, width, depth), jnp.bfloat16),
                pltpu.VMEM(block, jnp.bfloat16),
                pltpu.VMEM(block, jnp.bfloat16),
                pltpu.VMEM(block, jnp.bfloat16),
                pltpu.VMEM(block, jnp.bfloat16),
                pltpu.VMEM((tokens, depth), jnp.bfloat16),
                pltpu.VMEM((tokens, depth), jnp.float32),
                pltpu.VMEM((n_ra - 1, tokens, depth), jnp.float32),
                pltpu.VMEM((n, STAT_ROWS, tokens), jnp.float32),
                pltpu.VMEM((n, STAT_ROWS, tokens), jnp.float32),
            ]
            + [pltpu.SemaphoreType.DMA((chunks,))] * 7
            + [pltpu.SemaphoreType.DMA((2, n))] * 2
            + [pltpu.SemaphoreType.DMA((n_ra - 1,))] * 2,
            compiler_params=pltpu.CompilerParams(
                collective_id=0, has_side_effects=True, vmem_limit_bytes=64 * 1000 * 1024
            ),
        )(
            residual_in, gain_in.reshape(1, depth), shift_in.reshape(1, depth),
            gain_out.reshape(1, depth), shift_out.reshape(1, depth), up_weight, down_weight,
        )

    in_specs = (P("dp", "cb"), P("cb"), P("cb"), P("cb", "ra"), P("ra", "cb"), P("cb"), P("cb"))
    return jax.shard_map(
        per_device, mesh=mesh, in_specs=in_specs, out_specs=P("dp", "cb"), check_vma=False
    )
```

time: 338 us -> 124 us (0.37)
  waiting for transfers between devices: 244 us -> 0 us
  Pallas kernels: 0 us -> 122 us
  blocking collectives: 42.2 us -> 0 us
  matrix products: 26.3 us -> 0 us
  between operations: 13.2 us -> 0.01 us
  other arithmetic: 11.5 us -> 0 us
    reduce_scatter x1 -> x0, waiting for transfers between devices: 144 us -> none  [per_device(): share = lax.psum_scatter(products, 'cb', scatter_dimension=1, tiled=True)]
    pallas_call x0 -> x1, Pallas kernels: none -> 122 us  [per_device(): pl.pallas_call(functools.partial(kernel, n, n_ra), out_shape=jax.ShapeDty...]
    all_gather x1 -> x0, waiting for transfers between devices: 81.4 us -> none  [per_device(): lax.all_gather(hidden_share, 'cb', axis=1, tiled=True)]
    psum x4 -> x0, blocking collectives: 42.2 us -> none  [the longest x2 25.5 us: standardize(): sums = lax.psum(jnp.sum(values, axis=1), 'cb')]
    dot_general x2 -> x0, matrix products: 26.3 us -> none  [the longest x1 13.8 us: per_device(): products = jnp.dot(normed, up_weight, preferred_element_type=jnp.float32)]
    psum x1 -> x0, waiting for transfers between devices: 18.1 us -> none  [per_device(): branch = lax.psum(branch_part, 'ra')]
    reduce_sum x4 -> x0, other arithmetic: 5.9 us -> none  [the longest x2 3.05 us: standardize(): spread = lax.psum(jnp.sum(centred * centred, axis=1), 'cb') / count]
    convert_element_type x2 -> x0, other arithmetic: 5.59 us -> none  [the longest x1 2.8 us: per_device(): return (standardize(total) * gain_out + shift_out).astype(jnp.bfloat16)]
  transfers between devices with their start and end apart: 3 -> 0, of which waited for: 3 -> 0; matrix products, arithmetic and copies ran while one was open for 0% -> 0% of each run, Pallas kernels for 0% -> 0%
where the time goes in v1:
time: 124 us
  Pallas kernels  122 us (98%)
  local copies, waits for them, and re-layouts  1.87 us (2%)
    pallas_call x1, Pallas kernels, per_device(): pl.pallas_call(functools.partial(kernel, n, n_ra), out_shape=jax.ShapeDty...  122 us

profile of v1, /device:TPU:0, one launch (start us, length us, event | category | flops | bytes accessed | tf_op | source)
XLA Modules:
  0.0 123.6 jit_solution(14995305373039720799)
XLA Ops:
  0.0 121.7 %shard_map.73 = bf16[256,1024]{1,0:T(8,128)(2,1)} custom-call(bf16[256,1024]{1,0:T(8,128)(2,1)} %x_ref.1, f32[1,1024]{1,0:T(1,128)} %bitcast.4, f32[1,1024]{1,0:T(1,128)} %bitcast.5, f32[1,1024]{1,0:T(1,128)} %bitcast.6, f32[1,1024]{1,0:T(1,128)} %bitcast.7, bf16[1024,8192]{1,0:T(8,128)(2,1)} %up_hbm.1, bf16[8192,1024]{1,0:T(8,128)(2,1)} %down_hbm.1), custom_call_target="tpu_custom_call" | custom-call | tf_op jit(solution)/shard_map/pallas_call | solution.py:217
  121.7 1.9 %copy.9 = bf16[256,1024]{1,0:T(8,128)(2,1)} copy(bf16[256,1024]{1,0:T(8,128)(2,1)} %shard_map.73) | data formatting | bytes 1048576

commit v2 on v1

--- a/solution.py
+++ b/solution.py
@@ -11,14 +11,16 @@
 LANES = 128
 STAT_ROWS = 8
 CHUNK = 256
-WINDOW = 3
-LAG = 2
-LAG_STEP = 4
+WINDOW = 4
+LAG = 3
+AHEAD = 8
+SPLIT = 2
+LAG_STEP = 7
 
 
 def kernel(
     n, n_ra, x_ref, gain_in_ref, shift_in_ref, gain_out_ref, shift_out_ref, up_hbm, down_hbm, out_ref,
-    up_v, down_v, sums, from_outer, from_partner, hidden, normed, acc, acc_in, stats_in, stats_out,
+    up_v, down_v, tile_v, sums, from_outer, from_partner, hidden, normed, acc, acc_in, stats_in, stats_out,
     up_sem, down_sem, sums_sent, outer_got, partner_got, hidden_sent, hidden_got,
     stat_sent, stat_got, acc_sent, acc_got,
 ):
@@ -26,7 +28,10 @@
     ra = lax.axis_index("ra")
     chunks, depth, width = up_v.shape
     tokens = x_ref.shape[0]
+    steps, rows = sums.shape[0], sums.shape[1]
+    split = steps // chunks
     half = n // 2
+    ahead = min(AHEAD, chunks)
     side = me // half
     level = me * (1 - side) + (n - 1 - me) * side
     inner = lax.rem(me + 1 - 2 * side + n, n)
@@ -42,27 +47,21 @@
         rows = pl.ds(pl.multiple_of(c * width, width), width)
         return pltpu.make_async_copy(down_hbm.at[rows, :], down_v.at[c], down_sem.at[c])
 
-    @pl.loop(0, chunks)
-    def _(c):
-        up_copy(c).start()
-
-    @pl.loop(0, chunks)
-    def _(c):
-        down_copy(c).start()
-
     barrier = pltpu.get_barrier_semaphore()
     for k in range(1, n):
         pl.semaphore_signal(barrier, inc=1, device_id={"cb": lax.rem(me + k, n)}, device_id_type=MESH)
     for k in range(1, n_ra):
         pl.semaphore_signal(barrier, inc=1, device_id={"ra": lax.rem(ra + k, n_ra)}, device_id_type=MESH)
 
-    def local_stats(values, stats):
+    for c in range(ahead):
+        up_copy(c).start()
+
+    def row_stats(values):
         total = jnp.sum(values, axis=1, keepdims=True)
         centred = values - total * (1.0 / depth)
         squares = jnp.sum(centred * centred, axis=1, keepdims=True)
-        lane = lax.broadcasted_iota(jnp.int32, (tokens, LANES), 1)
-        tile = jnp.where(lane == 0, total, jnp.where(lane == 1, squares, 0.0))
-        stats[me] = tile.T[:STAT_ROWS]
+        lane = lax.broadcasted_iota(jnp.int32, (values.shape[0], LANES), 1)
+        return jnp.where(lane == 0, total, jnp.where(lane == 1, squares, 0.0))
 
     def stat_copy(stats, which, k, slot):
         return pltpu.make_async_remote_copy(
@@ -95,10 +94,12 @@
         return tile[:, 0:1], tile[:, 1:2]
 
     values = x_ref[...].astype(jnp.float32)
-    local_stats(values, stats_in)
+    stats_in[me] = row_stats(values).T[:STAT_ROWS]
     acc[...] = jnp.zeros_like(acc)
     pl.semaphore_wait(barrier, n - 1 + n_ra - 1)
     send_stats(stats_in, 0)
+    for c in range(ahead):
+        down_copy(c).start()
     mean, scale = merged_stats(stats_in, 0)
     normed[...] = (
         (x_ref[...].astype(jnp.float32) - mean) * scale * gain_in_ref[...] + shift_in_ref[...]
@@ -116,9 +117,29 @@
             recv_sem=hidden_got.at[c], device_id={"cb": outer}, device_id_type=MESH,
         )
 
+    def block_of(r):
+        return pl.ds(pl.multiple_of(r * rows, rows), rows)
+
+    def acc_copy(k, r):
+        return pltpu.make_async_remote_copy(
+            src_ref=acc.at[block_of(r)], dst_ref=acc_in.at[k - 1, block_of(r)],
+            send_sem=acc_sent.at[k - 1, r], recv_sem=acc_got.at[k - 1, r],
+            device_id={"ra": lax.rem(ra + k, n_ra)}, device_id_type=MESH,
+        )
+
     def inward(c):
-        up_copy(c).wait()
-        part = jnp.dot(normed[...], up_v[c], preferred_element_type=jnp.float32)
+        unit, r = c // split, lax.rem(c, split)
+
+        @pl.when(r == 0)
+        def _():
+            up_copy(unit).wait()
+
+            @pl.when(unit + ahead < chunks)
+            def _():
+                up_copy(unit + ahead).start()
+                down_copy(unit + ahead).start()
+
+        part = jnp.dot(normed[block_of(r)], up_v[unit], preferred_element_type=jnp.float32)
 
         @pl.when(has_outer)
         def _():
@@ -156,14 +177,24 @@
         def _():
             hidden_copy(c).start()
 
-        down_copy(c).wait()
-        acc[...] += jnp.dot(hidden[c], down_v[c], preferred_element_type=jnp.float32)
+        unit, r = c // split, lax.rem(c, split)
+
+        @pl.when(r == 0)
+        def _():
+            down_copy(unit).wait()
+
+        acc[block_of(r)] += jnp.dot(hidden[c], down_v[unit], preferred_element_type=jnp.float32)
+
+        @pl.when(unit == chunks - 1)
+        def _():
+            for k in range(1, n_ra):
+                acc_copy(k, r).start()
 
     lag = LAG + LAG_STEP * (half - 1 - level)
 
-    @pl.loop(0, chunks + lag)
+    @pl.loop(0, steps + lag)
     def _(step):
-        @pl.when(step < chunks)
+        @pl.when(step < steps)
         def _():
             inward(step)
 
@@ -171,33 +202,27 @@
         def _():
             outward(step - lag)
 
-    def acc_copy(k):
-        return pltpu.make_async_remote_copy(
-            src_ref=acc, dst_ref=acc_in.at[k - 1], send_sem=acc_sent.at[k - 1], recv_sem=acc_got.at[k - 1],
-            device_id={"ra": lax.rem(ra + k, n_ra)}, device_id_type=MESH,
-        )
-
-    for k in range(1, n_ra):
-        acc_copy(k).start()
-
-    @pl.loop(max(chunks - WINDOW, 0), chunks)
+    @pl.loop(max(steps - WINDOW, 0), steps)
     def _(c):
         sum_copy(c, from_outer, outer_got).wait_send()
 
     @pl.when(has_outer)
     def _():
-        @pl.loop(0, chunks)
+        @pl.loop(0, steps)
         def _(c):
             hidden_copy(c).wait_send()
 
-    for k in range(1, n_ra):
-        acc_copy(k).wait()
-    branch = acc[...]
-    for k in range(1, n_ra):
-        branch = branch + acc_in[k - 1]
-    total = 2.0**0.25 * normed[...].astype(jnp.float32) + branch
-    acc[...] = total
-    local_stats(total, stats_out)
+    for r in range(split):
+        block = pl.ds(r * rows, rows)
+        for k in range(1, n_ra):
+            acc_copy(k, r).wait()
+        branch = acc[block]
+        for k in range(1, n_ra):
+            branch = branch + acc_in[k - 1, block]
+        total = 2.0**0.25 * normed[block].astype(jnp.float32) + branch
+        acc[block] = total
+        tile_v[block] = row_stats(total)
+    stats_out[me] = tile_v[...].T[:STAT_ROWS]
     send_stats(stats_out, 1)
     mean, scale = merged_stats(stats_out, 1)
     out_ref[...] = ((acc[...] - mean) * scale * gain_out_ref[...] + shift_out_ref[...]).astype(jnp.bfloat16)
@@ -213,7 +238,8 @@
         chunks = units // width
         vmem = pl.BlockSpec(memory_space=pltpu.VMEM)
         hbm = pl.BlockSpec(memory_space=pl.ANY)
-        block = (chunks, tokens, width)
+        split = SPLIT if tokens % (SPLIT * LANES // 2) == 0 else 1
+        block = (chunks * split, tokens // split, width)
         return pl.pallas_call(
             functools.partial(kernel, n, n_ra),
             out_shape=jax.ShapeDtypeStruct((tokens, depth), jnp.bfloat16),
@@ -222,6 +248,7 @@
             scratch_shapes=[
                 pltpu.VMEM((chunks, depth, width), jnp.bfloat16),
                 pltpu.VMEM((chunks, width, depth), jnp.bfloat16),
+                pltpu.VMEM((tokens, LANES), jnp.float32),
                 pltpu.VMEM(block, jnp.bfloat16),
                 pltpu.VMEM(block, jnp.bfloat16),
                 pltpu.VMEM(block, jnp.bfloat16),
@@ -232,9 +259,10 @@
                 pltpu.VMEM((n, STAT_ROWS, tokens), jnp.float32),
                 pltpu.VMEM((n, STAT_ROWS, tokens), jnp.float32),
             ]
-            + [pltpu.SemaphoreType.DMA((chunks,))] * 7
+            + [pltpu.SemaphoreType.DMA((chunks,))] * 2
+            + [pltpu.SemaphoreType.DMA((chunks * split,))] * 5
             + [pltpu.SemaphoreType.DMA((2, n))] * 2
-            + [pltpu.SemaphoreType.DMA((n_ra - 1,))] * 2,
+            + [pltpu.SemaphoreType.DMA((n_ra - 1, split))] * 2,
             compiler_params=pltpu.CompilerParams(
                 collective_id=0, has_side_effects=True, vmem_limit_bytes=64 * 1000 * 1024
             ),

time: 124 us -> 121 us (0.976)
  Pallas kernels: 122 us -> 119 us
    pallas_call x1, Pallas kernels: 122 us -> 119 us  [per_device(): pl.pallas_call(functools.partial(kernel, n, n_ra), out_shape=jax.ShapeDty...]
where the time goes in v2:
time: 121 us
  Pallas kernels  119 us (98%)
  local copies, waits for them, and re-layouts  1.87 us (2%)
    pallas_call x1, Pallas kernels, per_device(): pl.pallas_call(functools.partial(kernel, n, n_ra), out_shape=jax.ShapeDty...  119 us

profile of v2, /device:TPU:0, one launch (start us, length us, event | category | flops | bytes accessed | tf_op | source)
XLA Modules:
  0.0 121.1 jit_solution(4374402515591965201)
XLA Ops:
  0.0 119.2 %shard_map.73 = bf16[256,1024]{1,0:T(8,128)(2,1)} custom-call(bf16[256,1024]{1,0:T(8,128)(2,1)} %x_ref.1, f32[1,1024]{1,0:T(1,128)} %bitcast.4, f32[1,1024]{1,0:T(1,128)} %bitcast.5, f32[1,1024]{1,0:T(1,128)} %bitcast.6, f32[1,1024]{1,0:T(1,128)} %bitcast.7, bf16[1024,8192]{1,0:T(8,128)(2,1)} %up_hbm.1, bf16[8192,1024]{1,0:T(8,128)(2,1)} %down_hbm.1), custom_call_target="tpu_custom_call" | custom-call | tf_op jit(solution)/shard_map/pallas_call | solution.py:243
  119.2 1.9 %copy.9 = bf16[256,1024]{1,0:T(8,128)(2,1)} copy(bf16[256,1024]{1,0:T(8,128)(2,1)} %shard_map.73) | data formatting | bytes 1048576
